TPU v7x, 32 devices: a whole 2x2x4 slice. The times are simulated.
32 devices in a mesh: sp: 16 (over z, y, x), tp: 2 (over core).
Axes of the slice: x: 2, y: 2, z: 4, core: 2. Of those that a mesh axis runs over, the one named last changes fastest.
Arguments:
- tokens: bfloat16 [4096, 2048], P('sp', 'tp'), may hold values from -6 to 6
- norm_gain: float32 [2, 2048], replicated, may hold values from 0.1 to 1.9
- w_bgate: bfloat16 [2, 2048, 2048], P(None, 'sp', 'tp'), may hold values from -0.125 to 0.125
- w_cgate: bfloat16 [2, 2048, 2048], P(None, 'sp', 'tp'), may hold values from -0.125 to 0.125
- w_value: bfloat16 [2, 2048, 2048], P(None, 'sp', 'tp'), may hold values from -0.125 to 0.125
- conv_taps: float32 [2, 3, 2048], replicated, may hold values from -3.5 to 3.5
- w_out: bfloat16 [2, 2048, 2048], P(None, 'sp', 'tp'), may hold values from -0.125 to 0.125
Outputs:
- mixed_out: bfloat16 [4096, 2048], P('sp', 'tp')
All inputs are finite; a program needn't handle non-finite values.
Results may differ from a plain program's by a relative error of at most 0.015.
Values may be sent and summed in bfloat16 or wider, within the bound.
A program may use at most 64 MiB of HBM per device.

v0:
```python
import jax
import jax.numpy as jnp
from jax import lax
from jax.sharding import PartitionSpec as P


def shifted(shard, axis, by):
    size = lax.axis_size(axis)
    pairs = [(i, i + by) for i in range(size) if 0 <= i + by < size]
    return lax.ppermute(shard, axis, pairs)


def normalize(current, gain_row):
    as_float = current.astype(jnp.float32)
    scale = lax.rsqrt(jnp.mean(as_float * as_float, axis=-1, keepdims=True) + 1e-06)
    return (as_float * scale * gain_row).astype(jnp.bfloat16)


def causal_taps(product, previous, taps):
    padded = jnp.concatenate([previous, product], axis=0)
    return taps[0] * padded[:-2] + taps[1] * padded[1:-1] + taps[2] * padded[2:]


def shards(tokens, norm_gain, w_bgate, w_cgate, w_value, conv_taps, w_out):
    channels = tokens.shape[1]
    depth = w_bgate.shape[0]
    taps_own = lax.dynamic_slice_in_dim(conv_taps, lax.axis_index("tp") * channels, channels, 2)
    gathered = (
        lax.all_gather(w_bgate, "sp", axis=1, tiled=True),
        lax.all_gather(w_cgate, "sp", axis=1, tiled=True),
        lax.all_gather(w_value, "sp", axis=1, tiled=True),
        lax.all_gather(w_out, "sp", axis=1, tiled=True),
    )
    fringe_rows = 0
    current = tokens
    row_count = current.shape[0]
    for layer_idx in range(depth):
        whole = lax.all_gather(current, "tp", axis=1, tiled=True)
        normed = normalize(whole, norm_gain[layer_idx])
        bgate = jnp.dot(normed, gathered[0][layer_idx], preferred_element_type=jnp.float32)
        cgate = jnp.dot(normed, gathered[1][layer_idx], preferred_element_type=jnp.float32)
        values = jnp.dot(normed, gathered[2][layer_idx], preferred_element_type=jnp.float32)
        bgate = lax.optimization_barrier(bgate.astype(jnp.bfloat16))
        cgate = lax.optimization_barrier(cgate.astype(jnp.bfloat16))
        values = lax.optimization_barrier(values.astype(jnp.bfloat16))
        product = cgate.astype(jnp.float32) * values.astype(jnp.float32)
        previous = shifted(product[row_count - 2 :], "sp", 1)
        mixed = causal_taps(product, previous, taps_own[layer_idx])
        gated = (bgate.astype(jnp.float32) * mixed).astype(jnp.bfloat16)
        gated_all = lax.all_gather(gated, "tp", axis=1, tiled=True)
        update = jnp.dot(gated_all, gathered[3][layer_idx], preferred_element_type=jnp.float32)
        current = (current.astype(jnp.float32) + update).astype(jnp.bfloat16)
    return current


def solution(mesh):
    return jax.shard_map(
        shards,
        mesh=mesh,
        in_specs=(
            P("sp", "tp"),
            P(),
            P(None, "sp", "tp"),
            P(None, "sp", "tp"),
            P(None, "sp", "tp"),
            P(),
            P(None, "sp", "tp"),
        ),
        out_specs=P("sp", "tp"),
        check_vma=False,
    )
```

profile of v0, /device:TPU:0, one launch (start us, length us, event | category | flops | bytes accessed | tf_op | source)
XLA Modules:
  0.0 537.6 jit_solution(7436233771248528411)
XLA Ops:
  6.5 0.7 all-gather.9.cloned.1.call-update
  7.3 0.7 all-gather.13.cloned.1.call-update
  8.1 0.7 all-gather.15.cloned.1.call-update
  8.8 0.5 all-gather.11.cloned.1.call-update
  9.4 0.5 all-gather.19.cloned.1.call-update
  10.0 0.1 constant_dynamic-slice_fusion.3
  10.1 10.6 %all-gather.9.cloned.1.call-done = bf16[256,2048]{1,0:T(8,128)(2,1)} async-done(((bf16[256,1024]{1,0:T(8,128)(2,1)}), bf16[256,2048]{1,0:T(8,128)(2,1)}) %all-gather.9.cloned.1.call-update) | async-done | bytes 1048592 | tf_op jit(solution)/shard_map/all_gather | solution.py:38
  20.7 1.5 fusion.8
  22.2 114.6 %all-gather.13.cloned.1.call-done = bf16[2,2048,1024]{2,1,0:T(8,128)(2,1)} async-done(((bf16[2,128,1024]{2,1,0:T(8,128)(2,1)}), bf16[2,2048,1024]{2,1,0:T(8,128)(2,1)}) %all-gather.13.cloned.1.call-update) | async-done | bytes 8388624 | tf_op jit(solution)/shard_map/all_gather | solution.py:30
  136.8 3.9 fusion.19
  140.7 109.3 %all-gather.15.cloned.1.call-done = bf16[2,2048,1024]{2,1,0:T(8,128)(2,1)} async-done(((bf16[2,128,1024]{2,1,0:T(8,128)(2,1)}), bf16[2,2048,1024]{2,1,0:T(8,128)(2,1)}) %all-gather.15.cloned.1.call-update) | async-done | bytes 8388624 | tf_op jit(solution)/shard_map/all_gather | solution.py:31
  250.0 3.5 fusion.20
  253.5 0.2 convert_multiply_fusion.5
  253.7 3.4 collective-permute-start
  257.1 106.0 %all-gather.11.cloned.1.call-done = bf16[2,2048,1024]{2,1,0:T(8,128)(2,1)} async-done(((bf16[2,128,1024]{2,1,0:T(8,128)(2,1)}), bf16[2,2048,1024]{2,1,0:T(8,128)(2,1)}) %all-gather.11.cloned.1.call-update) | async-done | bytes 8388624 | tf_op jit(solution)/shard_map/all_gather | solution.py:29
  363.0 3.5 fusion.18
  366.6 1.2 fusion.35
  367.8 0.0 all-gather.21.cloned.1.call-start
  367.8 108.2 %all-gather.19.cloned.1.call-done = bf16[2,2048,1024]{2,1,0:T(8,128)(2,1)} async-done(((bf16[2,128,1024]{2,1,0:T(8,128)(2,1)}), bf16[2,2048,1024]{2,1,0:T(8,128)(2,1)}) %all-gather.19.cloned.1.call-update) | async-done | bytes 8388624 | tf_op jit(solution)/shard_map/all_gather | solution.py:32
  476.0 8.7 %all-gather.17.cloned.1.call-done = bf16[256,2048]{1,0:T(8,128)(2,1)} async-done(((bf16[256,1024]{1,0:T(8,128)(2,1)}), bf16[256,2048]{1,0:T(8,128)(2,1)}) %all-gather.17.cloned.1.call-update) | async-done | bytes 1048592 | tf_op jit(solution)/shard_map/all_gather | solution.py:50
  484.7 4.6 fusion.17
  489.3 0.0 all-gather.23.cloned.1.call-start
  489.3 10.3 %all-gather.21.cloned.1.call-done = bf16[256,2048]{1,0:T(8,128)(2,1)} async-done(((bf16[256,1024]{1,0:T(8,128)(2,1)}), bf16[256,2048]{1,0:T(8,128)(2,1)}) %all-gather.21.cloned.1.call-update) | async-done | bytes 1048592 | tf_op jit(solution)/shard_map/all_gather | solution.py:38
  499.7 1.5 fusion.11
  501.2 4.0 fusion.22
  505.2 3.6 fusion.23
  508.8 0.2 convert_multiply_fusion.4
  509.0 3.6 collective-permute-start.1
  512.7 1.3 fusion.21
  514.1 1.2 fusion.29
  515.3 10.9 %all-gather.23.cloned.1.call-done = bf16[256,2048]{1,0:T(8,128)(2,1)} async-done(((bf16[256,1024]{1,0:T(8,128)(2,1)}), bf16[256,2048]{1,0:T(8,128)(2,1)}) %all-gather.23.cloned.1.call-update) | async-done | bytes 1048592 | tf_op jit(solution)/shard_map/all_gather | solution.py:50
  526.1 4.6 fusion.16
  (33 shorter events, 0.3 us)
Async XLA Ops:
  6.5 3.4 copy-start.5
  6.5 3.5 copy-start.4
  6.5 14.1 %all-gather.9.cloned.1.call-start = ((), (), s32[]{:S(2)}) async-start(), calls=%async_computation | async-start | bytes 1572864 | tf_op jit(solution)/shard_map/all_gather | solution.py:38
  7.3 129.6 %all-gather.13.cloned.1.call-start = ((), (), s32[]{:S(2)}) async-start(), calls=%async_computation.2 | async-start | bytes 8912896 | tf_op jit(solution)/shard_map/all_gather | solution.py:30
  8.0 242.0 %all-gather.15.cloned.1.call-start = ((), (), s32[]{:S(2)}) async-start(), calls=%async_computation.3 | async-start | bytes 8912896 | tf_op jit(solution)/shard_map/all_gather | solution.py:31
  8.7 354.3 %all-gather.11.cloned.1.call-start = ((), (), s32[]{:S(2)}) async-start(), calls=%async_computation.1 | async-start | bytes 8912896 | tf_op jit(solution)/shard_map/all_gather | solution.py:29
  9.3 466.7 %all-gather.19.cloned.1.call-start = ((), (), s32[]{:S(2)}) async-start(), calls=%async_computation.5 | async-start | bytes 8912896 | tf_op jit(solution)/shard_map/all_gather | solution.py:32
  9.9 474.8 %all-gather.17.cloned.1.call-start = ((), (), s32[]{:S(2)}) async-start(), calls=%async_computation.4 | async-start | bytes 1572864 | tf_op jit(solution)/shard_map/all_gather | solution.py:50
  136.8 113.2 %copy-start = (bf16[256,2048]{1,0:T(8,128)(2,1)S(1)}, bf16[256,2048]{1,0:T(8,128)(2,1)}, u32[]{:S(2)}) copy-start(bf16[256,2048]{1,0:T(8,128)(2,1)} %all-gather.9.cloned.1.call-done) | copy-start | bytes 3145732
  253.7 112.9 %collective-permute-start = (f32[2,1024]{1,0:T(2,128)S(1)}, f32[2,1024]{1,0:T(2,128)S(1)}, u32[]{:S(2)}, u32[]{:S(2)}) collective-permute-start(f32[2,1024]{1,0:T(2,128)S(1)} %slice.105), channel_id=1, source_target_pairs={{0,2},{2,4},{4,6},{6,8},{8,10},{10,12},{12,14},{14,16},{16,18},{18... | collective-permute-start | bytes 24584 | tf_op jit(solution)/shard_map/ppermute | solution.py:10
  366.5 118.2 %copy-start.2 = (bf16[256,1024]{1,0:T(8,128)(2,1)S(1)}, bf16[256,1024]{1,0:T(8,128)(2,1)}, u32[]{:S(2)}) copy-start(bf16[256,1024]{1,0:T(8,128)(2,1)} %param.7) | copy-start | bytes 1572868
  367.8 131.9 %all-gather.21.cloned.1.call-start = ((), (), s32[]{:S(2)}) async-start(), calls=%async_computation.6 | async-start | bytes 1572864 | tf_op jit(solution)/shard_map/all_gather | solution.py:38
  489.3 36.8 %all-gather.23.cloned.1.call-start = ((), (), s32[]{:S(2)}) async-start(), calls=%async_computation.7 | async-start | bytes 1572864 | tf_op jit(solution)/shard_map/all_gather | solution.py:50
  501.2 4.0 copy-start.1
  501.2 11.5 %slice-start = ((s8[8388608]{0:T(1024)(128)(4,1)}), s8[4194304]{0:T(1024)(128)(4,1)S(1)}, s32[]{:S(2)}) async-start(s8[8388608]{0:T(1024)(128)(4,1)} %bitcast.66), calls=%async_computation.8 | async-start | bytes 8388608
  505.2 7.5 %slice-start.1 = ((s8[8388608]{0:T(1024)(128)(4,1)}), s8[4194304]{0:T(1024)(128)(4,1)S(1)}, s32[]{:S(2)}) async-start(s8[8388608]{0:T(1024)(128)(4,1)} %bitcast.66), calls=%async_computation.9 | async-start | bytes 8388608
  509.0 5.0 collective-permute-start.1
  514.0 12.1 %copy-start.3 = (bf16[256,1024]{1,0:T(8,128)(2,1)S(1)}, bf16[256,1024]{1,0:T(8,128)(2,1)}, u32[]{:S(2)}) copy-start(bf16[256,1024]{1,0:T(8,128)(2,1)} %fusion.17) | copy-start | bytes 1572868
Sparse Core Ops, SparseCore 0:
  8.9 11.7 all-gather.8
  23.4 113.3 all-gather.12
  139.6 110.3 all-gather.14
  252.6 110.3 all-gather.10
  365.6 110.3 all-gather.18
  477.4 7.2 all-gather.16
  489.4 10.1 all-gather.20
  515.4 10.7 all-gather.22
where the time goes:
time: 538 us
  waiting for transfers between devices  482 us (90%)
  matrix products  28.9 us (5%)
  between operations  13.7 us (3%)
  starting transfers between devices  7.28 us (1%)
  other arithmetic  5.77 us (1%)
    all_gather x1, waiting for transfers between devices, shards(): lax.all_gather(w_cgate, 'sp', axis=1, tiled=True)  115 us
    all_gather x1, waiting for transfers between devices, shards(): lax.all_gather(w_value, 'sp', axis=1, tiled=True)  109 us
    all_gather x1, waiting for transfers between devices, shards(): lax.all_gather(w_out, 'sp', axis=1, tiled=True)  108 us
    all_gather x1, waiting for transfers between devices, shards(): lax.all_gather(w_bgate, 'sp', axis=1, tiled=True)  106 us
    all_gather x2, waiting for transfers between devices, shards(): whole = lax.all_gather(current, 'tp', axis=1, tiled=True)  20.9 us
    all_gather x2, waiting for transfers between devices, shards(): gated_all = lax.all_gather(gated, 'tp', axis=1, tiled=True)  19.5 us
  transfers between devices with their start and end apart: 10, of which 8 were waited for; matrix products, arithmetic and copies ran while one was open for 3% of the time, Pallas kernels for 0%

commit v1 on v0

v1 whole, which is shorter than its diff:
```python
import functools

import jax
import jax.numpy as jnp
from jax import lax
from jax.experimental import pallas as pl
from jax.experimental.pallas import tpu as pltpu
from jax.sharding import PartitionSpec as P

MESH = pl.DeviceIdType.MESH
LANES = 128
AHEAD = 2
F32 = jnp.float32
BF16 = jnp.bfloat16


def mixer_kernel(dims, tok, gain, wb, wc, wv, taps, wo, out,
                 acts, gates, normed, weights, product, cgate, result, landed,
                 loc_sem, plane_send, plane_recv, line_send, line_recv,
                 ag_send, ag_recv, pair_send, pair_recv,
                 halo_send, halo_recv, out_send, out_recv):
    depth, group, line, tps, rows, cols, width, krows = dims
    span = rows * group
    block = krows * group
    chunks = [(l, m) for l in range(depth) for m in range(4)]
    sources = (wc, wv, wb, wo)
    sp, t = lax.axis_index("sp"), lax.axis_index("tp")
    z, q = sp // group, sp % group
    own = pl.multiple_of(t * cols + q * width, width)
    tile = min(256, span)

    def in_plane(d):
        return (z * group + (q + d) % group, t)

    def in_pair(d):
        return (sp, (t + d) % tps)

    def remote(src, dst, send, recv, device):
        return pltpu.make_async_remote_copy(src_ref=src, dst_ref=dst, send_sem=send, recv_sem=recv,
                                            device_id=device, device_id_type=MESH)

    barrier = pltpu.get_barrier_semaphore()

    def hello(device):
        pl.semaphore_signal(barrier, inc=1, device_id=device, device_id_type=MESH)

    for d in range(1, group):
        hello(in_plane(d))
    for d in range(1, tps):
        hello(in_pair(d))

    @pl.when(z > 0)
    def _():
        hello((sp - group, t))

    @pl.when(z < line - 1)
    def _():
        hello((sp + group, t))

    pl.semaphore_wait(barrier, group - 1 + tps - 1
                      + jnp.where(z > 0, 1, 0) + jnp.where(z < line - 1, 1, 0))

    def weight_rows(i, zz, qq):
        l, m = chunks[i]
        return weights.at[l, m, pl.ds(pl.multiple_of((zz * group + qq) * krows, krows), krows), :]

    def weight_block(i, zz):
        l, m = chunks[i]
        return weights.at[l, m, pl.ds(pl.multiple_of(zz * block, block), block), :]

    def weight_source(i, qq):
        l, m = chunks[i]
        return sources[m].at[l, :, pl.ds(pl.multiple_of(qq * width, width), width)]

    def plane_copy(i, d, sender):
        return remote(weight_source(i, (q + d) % group), weight_rows(i, z, sender),
                      plane_send.at[i, d], plane_recv.at[i, d], in_plane(d))

    def local_copy(i):
        return pltpu.make_async_copy(weight_source(i, q), weight_rows(i, z, q), loc_sem.at[i])

    def line_copy(i, zz, up):
        blk = weight_block(i, zz)
        return remote(blk, blk, line_send.at[0 if up else 1, i, zz], line_recv.at[i, zz],
                      (sp + group, t) if up else (sp - group, t))

    def plane_start(i):
        local_copy(i).start()
        for d in range(1, group):
            plane_copy(i, d, q).start()

    def line_start(i):
        local_copy(i).wait()
        for d in range(1, group):
            plane_copy(i, d, (q + group - d) % group).wait_recv()

        @pl.when(z < line - 1)
        def _():
            line_copy(i, z, True).start()

        @pl.when(z > 0)
        def _():
            line_copy(i, z, False).start()

    def line_round(i):
        if i + AHEAD < len(chunks):
            line_start(i + AHEAD)

        def step(j, carry):
            below, above = z - 1 - j, z + 1 + j

            @pl.when(below >= 0)
            def _():
                line_copy(i, below, True).wait_recv()

                @pl.when(z < line - 1)
                def _():
                    line_copy(i, below, True).start()

            @pl.when(above < line)
            def _():
                line_copy(i, above, False).wait_recv()

                @pl.when(z > 0)
                def _():
                    line_copy(i, above, False).start()

            return carry

        lax.fori_loop(0, line - 1, step, 0)

    def act_slice(ph, tt, qq):
        l = ph // 2
        if ph == 0:
            return acts.at[0, pl.ds(pl.multiple_of(qq * rows, rows), rows),
                           pl.ds(pl.multiple_of(tt * cols, cols), cols)]
        buf = acts if ph % 2 == 0 else gates
        return buf.at[l, :, pl.ds(pl.multiple_of(tt * cols + qq * width, width), width)]

    def ag_copy(ph, d, qq):
        src = tok if ph == 0 else act_slice(ph, t, q)
        return remote(src, act_slice(ph, t, qq), ag_send.at[ph, d], ag_recv.at[ph, d], in_plane(d))

    def pair_copy(ph, dq, d, tt):
        qq = (q + group - dq) % group
        src = tok if ph == 0 and dq == 0 else act_slice(ph, t, qq)
        return remote(src, act_slice(ph, tt, qq), pair_send.at[ph, dq, d], pair_recv.at[ph, dq, d],
                      in_pair(d))

    def gather_start(ph):
        for d in range(1, group):
            ag_copy(ph, d, q).start()
        for d in range(1, tps):
            pair_copy(ph, 0, d, t).start()

    def gather_finish(ph):
        for d in range(1, group):
            ag_copy(ph, d, (q + group - d) % group).wait_recv()
            for e in range(1, tps):
                pair_copy(ph, d, e, t).start()
        for d in range(group):
            for e in range(1, tps):
                pair_copy(ph, d, e, (t + tps - e) % tps).wait_recv()

    def tiles(body):
        def step(i, carry):
            body(pl.multiple_of(i * tile, tile))
            return carry

        lax.fori_loop(0, span // tile, step, 0)

    def normalize(l):
        sub = 32

        def step(i, carry):
            at = pl.ds(pl.multiple_of(i * sub, sub), sub)
            x = acts[l, at, :].astype(F32)
            scale = lax.rsqrt(jnp.mean(x * x, axis=-1, keepdims=True) + 1e-06)
            normed[at, :] = (x * scale * gain[pl.ds(l, 1), :]).astype(BF16)
            return carry

        lax.fori_loop(0, span // sub, step, 0)

    def project(l, m, r):
        return jnp.dot(normed[pl.ds(r, tile), :], weights[l, m], preferred_element_type=F32).astype(BF16)

    def halo_copy(l):
        return remote(product.at[l, pl.ds(span, 8), :], product.at[l, pl.ds(0, 8), :],
                      halo_send.at[l], halo_recv.at[l], (sp + group, t))

    def do_cgate(l):
        def body(r):
            cgate[pl.ds(r, tile), :] = project(l, 0, r)
        tiles(body)

    def do_values(l):
        def body(r):
            values = project(l, 1, r)
            product[l, pl.ds(r + 8, tile), :] = cgate[pl.ds(r, tile), :].astype(F32) * values.astype(F32)
        tiles(body)

        @pl.when(z < line - 1)
        def _():
            halo_copy(l).start()

    def do_bgate(l):
        @pl.when(z > 0)
        def _():
            halo_copy(l).wait_recv()

        @pl.when(z == 0)
        def _():
            product[l, pl.ds(0, 8), :] = jnp.zeros((8, width), F32)

        tap = [taps[l, pl.ds(k, 1), pl.ds(own, width)] for k in range(3)]

        def body(r):
            bgate = project(l, 2, r).astype(F32)
            near = product[l, pl.ds(r, tile + 8), :]
            mixed = tap[0] * near[6:6 + tile] + tap[1] * near[7:7 + tile] + tap[2] * near[8:8 + tile]
            gates[l, pl.ds(r, tile), pl.ds(own, width)] = (bgate * mixed).astype(BF16)
        tiles(body)

    def do_out(l):
        def body(r):
            update = jnp.dot(gates[l, pl.ds(r, tile), :], weights[l, 3], preferred_element_type=F32)
            current = (acts[l, pl.ds(r, tile), pl.ds(own, width)].astype(F32) + update).astype(BF16)
            if l + 1 < depth:
                acts[l + 1, pl.ds(r, tile), pl.ds(own, width)] = current
            else:
                result[pl.ds(r, tile), :] = current
        tiles(body)

    def out_copy(d, qq):
        return remote(result.at[pl.ds(pl.multiple_of((q + d) % group * rows, rows), rows), :],
                      landed.at[:, pl.ds(pl.multiple_of(qq * width, width), width)],
                      out_send.at[d], out_recv.at[d], in_plane(d))

    own_tokens = pltpu.make_async_copy(tok, act_slice(0, t, q), loc_sem.at[len(chunks)])
    plane_start(0)
    own_tokens.start()
    gather_start(0)
    for i in range(1, len(chunks)):
        plane_start(i)
    for i in range(min(AHEAD, len(chunks))):
        line_start(i)
    for l in range(depth):
        line_round(4 * l)
        if l == 0:
            own_tokens.wait()
        gather_finish(2 * l)
        normalize(l)
        do_cgate(l)
        line_round(4 * l + 1)
        do_values(l)
        line_round(4 * l + 2)
        do_bgate(l)
        gather_start(2 * l + 1)
        line_round(4 * l + 3)
        gather_finish(2 * l + 1)
        do_out(l)
        if l + 1 < depth:
            gather_start(2 * l + 2)
    for d in range(1, group):
        out_copy(d, q).start()
    landed[:, pl.ds(pl.multiple_of(q * width, width), width)] = result[
        pl.ds(pl.multiple_of(q * rows, rows), rows), :]
    for d in range(1, group):
        out_copy(d, (q + group - d) % group).wait_recv()
    out[...] = landed[...]

    for i in range(len(chunks)):
        for d in range(1, group):
            plane_copy(i, d, q).wait_send()

        def step(zz, carry):
            @pl.when((z < line - 1) & (zz <= z))
            def _():
                line_copy(i, zz, True).wait_send()

            @pl.when((z > 0) & (zz >= z))
            def _():
                line_copy(i, zz, False).wait_send()

            return carry

        lax.fori_loop(0, line, step, 0)
    for ph in range(2 * depth):
        for d in range(1, group):
            ag_copy(ph, d, q).wait_send()
        for d in range(group):
            for e in range(1, tps):
                pair_copy(ph, d, e, t).wait_send()
    for l in range(depth):
        @pl.when(z < line - 1)
        def _():
            halo_copy(l).wait_send()
    for d in range(1, group):
        out_copy(d, q).wait_send()


def shards(sp_size, tps, tokens, norm_gain, w_bgate, w_cgate, w_value, conv_taps, w_out):
    rows, cols = tokens.shape
    depth, krows, _ = w_bgate.shape
    group = 4
    while group > 1 and (sp_size % group or cols % (group * LANES)):
        group //= 2
    line = sp_size // group
    width = cols // group
    span = rows * group
    full = krows * sp_size
    n = 4 * depth
    dims = (depth, group, line, tps, rows, cols, width, krows)
    anywhere = pl.BlockSpec(memory_space=pl.ANY)
    vmem = pl.BlockSpec(memory_space=pltpu.VMEM)
    dma = pltpu.SemaphoreType.DMA
    return pl.pallas_call(
        functools.partial(mixer_kernel, dims),
        out_shape=jax.ShapeDtypeStruct((rows, cols), BF16),
        in_specs=[anywhere, vmem, anywhere, anywhere, anywhere, vmem, anywhere],
        out_specs=vmem,
        scratch_shapes=[
            pltpu.VMEM((depth, span, full), BF16),
            pltpu.VMEM((depth, span, full), BF16),
            pltpu.VMEM((span, full), BF16),
            pltpu.VMEM((depth, 4, full, width), BF16),
            pltpu.VMEM((depth, span + 8, width), F32),
            pltpu.VMEM((span, width), BF16),
            pltpu.VMEM((span, width), BF16),
            pltpu.VMEM((rows, cols), BF16),
            dma((n + 1,)), dma((n, group)), dma((n, group)),
            dma((2, n, line)), dma((n, line)),
            dma((2 * depth, group)), dma((2 * depth, group)),
            dma((2 * depth, group, tps)), dma((2 * depth, group, tps)),
            dma((depth,)), dma((depth,)), dma((group,)), dma((group,)),
        ],
        compiler_params=pltpu.CompilerParams(
            collective_id=0, has_side_effects=True, vmem_limit_bytes=60 * 1024 * 1024),
    )(tokens, norm_gain, w_bgate, w_cgate, w_value, conv_taps, w_out)


def solution(mesh):
    return jax.shard_map(
        functools.partial(shards, mesh.shape["sp"], mesh.shape["tp"]),
        mesh=mesh,
        in_specs=(
            P("sp", "tp"),
            P(),
            P(None, "sp", "tp"),
            P(None, "sp", "tp"),
            P(None, "sp", "tp"),
            P(),
            P(None, "sp", "tp"),
        ),
        out_specs=P("sp", "tp"),
        check_vma=False,
    )
```

time: 538 us -> 227 us (0.42)
  waiting for transfers between devices: 482 us -> 0 us
  Pallas kernels: 0 us -> 224 us
  matrix products: 28.9 us -> 0 us
  between operations: 13.7 us -> 0.01 us
  starting transfers between devices: 7.28 us -> 0 us
  other arithmetic: 5.77 us -> 0 us
    all_gather x8 -> x0, waiting for transfers between devices: 478 us -> none  [the longest x1 115 us: shards(): lax.all_gather(w_cgate, 'sp', axis=1, tiled=True)]
    pallas_call x0 -> x1, Pallas kernels: none -> 224 us  [shards(): pl.pallas_call(functools.partial(mixer_kernel, dims), out_shape=jax.Shape...]
    dot_general x8 -> x0, matrix products: 28.9 us -> none  [the longest x2 9.14 us: shards(): jnp.dot(gated_all, gathered[3][layer_idx], preferred_element_type=jnp.flo...]
    ppermute x2 -> x0, starting transfers between devices: 7 us -> none  [shifted(): return lax.ppermute(shard, axis, pairs)]
  transfers between devices with their start and end apart: 10 -> 0, of which waited for: 8 -> 0; matrix products, arithmetic and copies ran while one was open for 3% -> 0% of each run, Pallas kernels for 0% -> 0%
where the time goes in v1:
time: 227 us
  Pallas kernels  224 us (99%)
  local copies, waits for them, and re-layouts  3.33 us (1%)
    pallas_call x1, Pallas kernels, shards(): pl.pallas_call(functools.partial(mixer_kernel, dims), out_shape=jax.Shape...  224 us

profile of v1, /device:TPU:0, one launch (start us, length us, event | category | flops | bytes accessed | tf_op | source)
XLA Modules:
  0.0 227.0 jit_solution(15712225392575991704)
XLA Ops:
  0.0 1.5 copy.8.taps
  1.5 223.7 %shard_map.73 = bf16[256,1024]{1,0:T(8,128)(2,1)} custom-call(bf16[256,1024]{1,0:T(8,128)(2,1)} %tok.1, f32[2,2048]{1,0:T(2,128)} %gain.1, bf16[2,128,1024]{2,1,0:T(8,128)(2,1)} %wb.1, bf16[2,128,1024]{2,1,0:T(8,128)(2,1)} %wc.1, bf16[2,128,1024]{2,1,0:T(8,128)(2,1)} %wv.1, f32[2,3,2048]{2,1,0:T(4,128)} %copy.8.taps, bf16[2,128,1024]{2,1,0:T(8,128)(2,1)} %wo.1), custom_call_target="tpu_custom_call" | custom-call | tf_op jit(solution)/shard_map/pallas_call | solution.py:317
  225.2 1.9 copy.10

commit v2 on v1

--- a/solution.py
+++ b/solution.py
@@ -10,6 +10,7 @@
 MESH = pl.DeviceIdType.MESH
 LANES = 128
 AHEAD = 2
+BEFORE_TOKENS = 2
 F32 = jnp.float32
 BF16 = jnp.bfloat16
 
@@ -27,7 +28,7 @@
     sp, t = lax.axis_index("sp"), lax.axis_index("tp")
     z, q = sp // group, sp % group
     own = pl.multiple_of(t * cols + q * width, width)
-    tile = min(256, span)
+    tile = min(256, rows)
 
     def in_plane(d):
         return (z * group + (q + d) % group, t)
@@ -103,9 +104,6 @@
             line_copy(i, z, False).start()
 
     def line_round(i):
-        if i + AHEAD < len(chunks):
-            line_start(i + AHEAD)
-
         def step(j, carry):
             below, above = z - 1 - j, z + 1 + j
 
@@ -128,39 +126,81 @@
             return carry
 
         lax.fori_loop(0, line - 1, step, 0)
-
-    def act_slice(ph, tt, qq):
-        l = ph // 2
+        if i + AHEAD < len(chunks):
+            line_start(i + AHEAD)
+
+    def act_half(ph, tt, qq, h):
         if ph == 0:
-            return acts.at[0, pl.ds(pl.multiple_of(qq * rows, rows), rows),
+            part = rows // 2
+            return acts.at[0, pl.ds(pl.multiple_of(qq * rows + h * part, part), part),
                            pl.ds(pl.multiple_of(tt * cols, cols), cols)]
+        part = span // 2
         buf = acts if ph % 2 == 0 else gates
-        return buf.at[l, :, pl.ds(pl.multiple_of(tt * cols + qq * width, width), width)]
-
-    def ag_copy(ph, d, qq):
-        src = tok if ph == 0 else act_slice(ph, t, q)
-        return remote(src, act_slice(ph, t, qq), ag_send.at[ph, d], ag_recv.at[ph, d], in_plane(d))
-
-    def pair_copy(ph, dq, d, tt):
-        qq = (q + group - dq) % group
-        src = tok if ph == 0 and dq == 0 else act_slice(ph, t, qq)
-        return remote(src, act_slice(ph, tt, qq), pair_send.at[ph, dq, d], pair_recv.at[ph, dq, d],
-                      in_pair(d))
+        return buf.at[ph // 2, pl.ds(h * part, part),
+                      pl.ds(pl.multiple_of(tt * cols + qq * width, width), width)]
+
+    def own_half(ph, h):
+        if ph == 0:
+            return tok.at[pl.ds(h * (rows // 2), rows // 2), :]
+        return act_half(ph, t, q, h)
+
+    def flip(qq, bits):
+        if bits & 1:
+            qq = qq + 1 - 2 * (qq % 2)
+        if bits & 2:
+            qq = qq + 2 - 4 * ((qq // 2) % 2)
+        return qq
+
+    directs = ([(1, 0), (1, 1)] if group >= 2 else []) + ([(2, 1), (2, 0)] if group >= 4 else [])
+    relays = [(1, 0, 2), (2, 1, 1)] if group >= 4 else []
+
+    def direct_copy(ph, bits, h, sending):
+        src = own_half(ph, h)
+        dst = act_half(ph, t, q if sending else flip(q, bits), h)
+        return remote(src, dst, ag_send.at[ph, bits, h], ag_recv.at[ph, bits, h],
+                      (z * group + flip(q, bits), t))
+
+    def relay_copy(ph, origin, h, to, sending):
+        part = act_half(ph, t, flip(q, origin if sending else 3), h)
+        return remote(part, part, ag_send.at[ph, 3, h], ag_recv.at[ph, 3, h],
+                      (z * group + flip(q, to), t))
+
+    def pair_copy(ph, bits, h, d, tt):
+        qq = flip(q, bits)
+        src = own_half(ph, h) if bits == 0 else act_half(ph, t, qq, h)
+        return remote(src, act_half(ph, tt, qq, h), pair_send.at[ph, bits, h, d],
+                      pair_recv.at[ph, bits, h, d], in_pair(d))
+
+    def pair_start(ph, bits, h):
+        for d in range(1, tps):
+            pair_copy(ph, bits, h, d, t).start()
 
     def gather_start(ph):
-        for d in range(1, group):
-            ag_copy(ph, d, q).start()
-        for d in range(1, tps):
-            pair_copy(ph, 0, d, t).start()
+        for bits, h in directs:
+            direct_copy(ph, bits, h, True).start()
+        for h in range(2):
+            pair_start(ph, 0, h)
+
+    def gather_relay(ph):
+        for origin, h, to in relays:
+            direct_copy(ph, origin, h, False).wait_recv()
+            relay_copy(ph, origin, h, to, True).start()
+        for origin, h, to in relays:
+            pair_start(ph, origin, h)
 
     def gather_finish(ph):
-        for d in range(1, group):
-            ag_copy(ph, d, (q + group - d) % group).wait_recv()
-            for e in range(1, tps):
-                pair_copy(ph, d, e, t).start()
-        for d in range(group):
-            for e in range(1, tps):
-                pair_copy(ph, d, e, (t + tps - e) % tps).wait_recv()
+        relayed = [(origin, h) for origin, h, _ in relays]
+        for bits, h in directs:
+            if (bits, h) not in relayed:
+                direct_copy(ph, bits, h, False).wait_recv()
+                pair_start(ph, bits, h)
+        for origin, h, to in relays:
+            relay_copy(ph, origin, h, to, False).wait_recv()
+            pair_start(ph, 3, h)
+        for bits in range(group):
+            for h in range(2):
+                for d in range(1, tps):
+                    pair_copy(ph, bits, h, d, (t + tps - d) % tps).wait_recv()
 
     def tiles(body):
         def step(i, carry):
@@ -221,7 +261,7 @@
             gates[l, pl.ds(r, tile), pl.ds(own, width)] = (bgate * mixed).astype(BF16)
         tiles(body)
 
-    def do_out(l):
+    def out_tile(l):
         def body(r):
             update = jnp.dot(gates[l, pl.ds(r, tile), :], weights[l, 3], preferred_element_type=F32)
             current = (acts[l, pl.ds(r, tile), pl.ds(own, width)].astype(F32) + update).astype(BF16)
@@ -229,40 +269,56 @@
                 acts[l + 1, pl.ds(r, tile), pl.ds(own, width)] = current
             else:
                 result[pl.ds(r, tile), :] = current
-        tiles(body)
+        return body
+
+    def do_out(l):
+        tiles(out_tile(l))
+
+    def do_out_rows(l, qq):
+        body = out_tile(l)
+        for k in range(rows // tile):
+            body(pl.multiple_of(qq * rows + k * tile, tile))
 
     def out_copy(d, qq):
         return remote(result.at[pl.ds(pl.multiple_of((q + d) % group * rows, rows), rows), :],
                       landed.at[:, pl.ds(pl.multiple_of(qq * width, width), width)],
                       out_send.at[d], out_recv.at[d], in_plane(d))
 
-    own_tokens = pltpu.make_async_copy(tok, act_slice(0, t, q), loc_sem.at[len(chunks)])
-    plane_start(0)
+    own_tokens = pltpu.make_async_copy(tok, acts.at[0, pl.ds(pl.multiple_of(q * rows, rows), rows), pl.ds(pl.multiple_of(t * cols, cols), cols)], loc_sem.at[len(chunks)])
     own_tokens.start()
-    gather_start(0)
-    for i in range(1, len(chunks)):
+    for i in range(len(chunks)):
+        if i == min(BEFORE_TOKENS, len(chunks) - 1):
+            gather_start(0)
         plane_start(i)
     for i in range(min(AHEAD, len(chunks))):
         line_start(i)
+    line_round(0)
+    gather_relay(0)
+    own_tokens.wait()
     for l in range(depth):
-        line_round(4 * l)
-        if l == 0:
-            own_tokens.wait()
         gather_finish(2 * l)
         normalize(l)
         do_cgate(l)
-        line_round(4 * l + 1)
+        if l == 0:
+            line_round(1)
         do_values(l)
         line_round(4 * l + 2)
         do_bgate(l)
         gather_start(2 * l + 1)
+        gather_relay(2 * l + 1)
         line_round(4 * l + 3)
+        if l + 1 < depth:
+            line_round(4 * l + 4)
         gather_finish(2 * l + 1)
-        do_out(l)
         if l + 1 < depth:
+            do_out(l)
             gather_start(2 * l + 2)
-    for d in range(1, group):
-        out_copy(d, q).start()
+            gather_relay(2 * l + 2)
+            line_round(4 * l + 5)
+    for d in range(1, group + 1):
+        do_out_rows(depth - 1, (q + d) % group)
+        if d > 1:
+            out_copy(d - 1, q).start()
     landed[:, pl.ds(pl.multiple_of(q * width, width), width)] = result[
         pl.ds(pl.multiple_of(q * rows, rows), rows), :]
     for d in range(1, group):
@@ -286,11 +342,14 @@
 
         lax.fori_loop(0, line, step, 0)
     for ph in range(2 * depth):
-        for d in range(1, group):
-            ag_copy(ph, d, q).wait_send()
-        for d in range(group):
-            for e in range(1, tps):
-                pair_copy(ph, d, e, t).wait_send()
+        for bits, h in directs:
+            direct_copy(ph, bits, h, True).wait_send()
+        for origin, h, to in relays:
+            relay_copy(ph, origin, h, to, True).wait_send()
+        for bits in range(group):
+            for h in range(2):
+                for d in range(1, tps):
+                    pair_copy(ph, bits, h, d, t).wait_send()
     for l in range(depth):
         @pl.when(z < line - 1)
         def _():
@@ -330,8 +389,8 @@
             pltpu.VMEM((rows, cols), BF16),
             dma((n + 1,)), dma((n, group)), dma((n, group)),
             dma((2, n, line)), dma((n, line)),
-            dma((2 * depth, group)), dma((2 * depth, group)),
-            dma((2 * depth, group, tps)), dma((2 * depth, group, tps)),
+            dma((2 * depth, 4, 2)), dma((2 * depth, 4, 2)),
+            dma((2 * depth, group, 2, tps)), dma((2 * depth, group, 2, tps)),
             dma((depth,)), dma((depth,)), dma((group,)), dma((group,)),
         ],
         compiler_params=pltpu.CompilerParams(

time: 227 us -> 192 us (0.85)
  Pallas kernels: 224 us -> 189 us
    pallas_call x1, Pallas kernels: 224 us -> 189 us  [shards(): pl.pallas_call(functools.partial(mixer_kernel, dims), out_shape=jax.Shape...]
where the time goes in v2:
time: 192 us
  Pallas kernels  189 us (98%)
  local copies, waits for them, and re-layouts  3.33 us (2%)
    pallas_call x1, Pallas kernels, shards(): pl.pallas_call(functools.partial(mixer_kernel, dims), out_shape=jax.Shape...  189 us

profile of v2, /device:TPU:0, one launch (start us, length us, event | category | flops | bytes accessed | tf_op | source)
XLA Modules:
  0.0 192.2 jit_solution(1363035327214837216)
XLA Ops:
  0.0 1.5 copy.8.taps
  1.5 188.8 %shard_map.73 = bf16[256,1024]{1,0:T(8,128)(2,1)} custom-call(bf16[256,1024]{1,0:T(8,128)(2,1)} %tok.1, f32[2,2048]{1,0:T(2,128)} %gain.1, bf16[2,128,1024]{2,1,0:T(8,128)(2,1)} %wb.1, bf16[2,128,1024]{2,1,0:T(8,128)(2,1)} %wc.1, bf16[2,128,1024]{2,1,0:T(8,128)(2,1)} %wv.1, f32[2,3,2048]{2,1,0:T(4,128)} %copy.8.taps, bf16[2,128,1024]{2,1,0:T(8,128)(2,1)} %wo.1), custom_call_target="tpu_custom_call" | custom-call | tf_op jit(solution)/shard_map/pallas_call | solution.py:376
  190.3 1.9 copy.10

commit v3 on v2

--- a/solution.py
+++ b/solution.py
@@ -126,8 +126,10 @@
             return carry
 
         lax.fori_loop(0, line - 1, step, 0)
-        if i + AHEAD < len(chunks):
+        if i + AHEAD < len(chunks) - 1:
             line_start(i + AHEAD)
+        if i == len(chunks) - 2:
+            line_start(i + 1)
 
     def act_half(ph, tt, qq, h):
         if ph == 0:
@@ -210,7 +212,7 @@
         lax.fori_loop(0, span // tile, step, 0)
 
     def normalize(l):
-        sub = 32
+        sub = 128
 
         def step(i, carry):
             at = pl.ds(pl.multiple_of(i * sub, sub), sub)
@@ -307,11 +309,10 @@
         gather_start(2 * l + 1)
         gather_relay(2 * l + 1)
         line_round(4 * l + 3)
-        if l + 1 < depth:
-            line_round(4 * l + 4)
         gather_finish(2 * l + 1)
         if l + 1 < depth:
             do_out(l)
+            line_round(4 * l + 4)
             gather_start(2 * l + 2)
             gather_relay(2 * l + 2)
             line_round(4 * l + 5)

time: 192 us -> 187 us (0.974)
  Pallas kernels: 189 us -> 183 us
    pallas_call x1, Pallas kernels: 189 us -> 183 us  [shards(): pl.pallas_call(functools.partial(mixer_kernel, dims), out_shape=jax.Shape...]
where the time goes in v3:
time: 187 us; the launch traced here: 186 us
  Pallas kernels  183 us (98%)
  local copies, waits for them, and re-layouts  3.33 us (2%)
    pallas_call x1, Pallas kernels, shards(): pl.pallas_call(functools.partial(mixer_kernel, dims), out_shape=jax.Shape...  183 us

profile of v3, /device:TPU:0, one launch (start us, length us, event | category | flops | bytes accessed | tf_op | source)
XLA Modules:
  0.0 186.3 jit_solution(6244033114683298686)
XLA Ops:
  0.0 1.5 copy.8.taps
  1.5 183.0 %shard_map.73 = bf16[256,1024]{1,0:T(8,128)(2,1)} custom-call(bf16[256,1024]{1,0:T(8,128)(2,1)} %tok.1, f32[2,2048]{1,0:T(2,128)} %gain.1, bf16[2,128,1024]{2,1,0:T(8,128)(2,1)} %wb.1, bf16[2,128,1024]{2,1,0:T(8,128)(2,1)} %wc.1, bf16[2,128,1024]{2,1,0:T(8,128)(2,1)} %wv.1, f32[2,3,2048]{2,1,0:T(4,128)} %copy.8.taps, bf16[2,128,1024]{2,1,0:T(8,128)(2,1)} %wo.1), custom_call_target="tpu_custom_call" | custom-call | tf_op jit(solution)/shard_map/pallas_call | solution.py:377
  184.4 1.9 %copy.10 = bf16[256,1024]{1,0:T(8,128)(2,1)} copy(bf16[256,1024]{1,0:T(8,128)(2,1)} %shard_map.73) | data formatting | bytes 1048576
